TPU v7x, 32 devices: a whole 2x2x4 slice. The times are simulated.
32 devices in a mesh: sp: 16 (over z, y, core), tp: 2 (over x).
Axes of the slice: x: 2, y: 2, z: 4, core: 2. Of those that a mesh axis runs over, the one named last changes fastest.
Arguments:
- target: bfloat16 [2048, 2048], P('sp'), may hold values from -0.375 to 0.375
- source: bfloat16 [4096, 2048], P(('sp', 'tp')), may hold values from -0.375 to 0.375
- target_gain: float32 [2048], replicated, may hold values from 0.3 to 12
- source_gain: float32 [2048], replicated, may hold values from 0.3 to 12
- w_query: bfloat16 [2048, 1024], P(None, 'tp'), may hold values from -0.125 to 0.125
- w_key: bfloat16 [2048, 256], replicated, may hold values from -0.125 to 0.125
- w_value: bfloat16 [2048, 256], replicated, may hold values from -0.125 to 0.125
- attended: bfloat16 [2048, 1024], P('sp', 'tp'), may hold values from -6 to 6
- d_attended: bfloat16 [2048, 1024], P('sp', 'tp'), may hold values from -24 to 24
Outputs:
- d_target: bfloat16 [2048, 2048], P('sp')
- d_source: float32 [4096, 2048], P(('sp', 'tp'))
- d_w_query: float32 [2048, 1024], P('sp', 'tp')
All inputs are finite; a program needn't handle non-finite values.
Results may differ from a plain program's by a relative error of at most 0.02.
The roundings to bfloat16 on the way count: a program that leaves them out, or rounds other values in their place, can miss the bound.
Values may be sent and summed in bfloat16 or wider, within the bound.
A program may use at most 64 MiB of HBM per device.

v0:
```python
import jax
import jax.numpy as jnp
from jax import lax
from jax.sharding import PartitionSpec as P

KVH = 2
HD = 128
EPS = 1e-06


def merged(shard, axis, combine):
    everything = jax.tree.map(lambda part: lax.all_gather(part, axis), shard)
    leading = jax.tree.map(lambda part: part[0], everything)

    def turn(k, so_far):
        return combine(so_far, jax.tree.map(lambda part: part[k], everything))

    return lax.fori_loop(1, lax.axis_size(axis), turn, leading)


def norm_rows(matrix, gain_vector):
    widened = matrix.astype(jnp.float32)
    inverse = lax.rsqrt(jnp.mean(widened * widened, axis=-1, keepdims=True) + EPS)
    return widened * inverse * gain_vector


def norm_back(matrix, gain_vector, cotangent):
    _, pullback = jax.vjp(lambda values: norm_rows(values, gain_vector), matrix.astype(jnp.float32))
    return pullback(cotangent)[0]


def block_count(row_count, most_rows):
    number = 1
    while row_count % (number * 2) == 0 and row_count // number > most_rows:
        number = number * 2
    return number


def merge_totals(earlier, latter):
    maxima = jnp.maximum(earlier[0], latter[0])
    totals = earlier[1] * jnp.exp(earlier[0] - maxima) + latter[1] * jnp.exp(latter[0] - maxima)
    return (maxima, totals)


def block_totals(queries, key_head, scaling):
    row_count = queries.shape[0]
    per_head = queries.reshape(row_count, -1, key_head.shape[1])
    scores = (
        jnp.einsum("rhd,sd->rhs", per_head, key_head, preferred_element_type=jnp.float32) * scaling
    )
    maxima = jnp.max(scores, axis=-1)
    totals = jnp.sum(jnp.exp(scores - maxima[..., None]), axis=-1)
    return (maxima, totals)


def score_grads(query_heads, grad_heads, delta_rows, log_total, key_head, value_head, scaling):
    scores = (
        jnp.einsum("rhd,sd->rhs", query_heads, key_head, preferred_element_type=jnp.float32)
        * scaling
    )
    weights = jnp.exp(scores - log_total[..., None])
    d_weights = jnp.einsum(
        "rhd,sd->rhs", grad_heads, value_head, preferred_element_type=jnp.float32
    )
    d_scores = (weights * (d_weights - delta_rows.astype(jnp.float32)[..., None])).astype(
        jnp.bfloat16
    )
    return (weights, d_scores)


def gradient_block(carried, blocks, key_head, value_head, scaling):
    key_acc, value_acc = carried
    queries, cotangent, delta_rows, log_total = blocks
    row_count = queries.shape[0]
    head_dim = key_head.shape[1]
    query_heads = queries.reshape(row_count, -1, head_dim)
    grad_heads = cotangent.reshape(row_count, -1, head_dim)
    weights, d_scores = score_grads(
        query_heads, grad_heads, delta_rows, log_total, key_head, value_head, scaling
    )
    key_acc = (
        key_acc
        + jnp.einsum("rhs,rhd->sd", d_scores, query_heads, preferred_element_type=jnp.float32)
        * scaling
    )
    value_acc = value_acc + jnp.einsum(
        "rhs,rhd->sd", weights.astype(jnp.bfloat16), grad_heads, preferred_element_type=jnp.float32
    )
    return ((key_acc, value_acc), None)


def local(target, source, target_gain, source_gain, w_query, w_key, w_value, attended, d_attended):
    tp_size = lax.axis_size("tp")
    local_rows = target.shape[0]
    source_rows = source.shape[0]
    query_width = w_query.shape[1]
    scaling = HD ** (-0.5)
    normed_target = norm_rows(target, target_gain).astype(jnp.bfloat16)
    normed_source = norm_rows(source, source_gain).astype(jnp.bfloat16)
    query = jnp.dot(normed_target, w_query, preferred_element_type=jnp.float32).astype(jnp.bfloat16)
    key_own = jnp.dot(normed_source, w_key, preferred_element_type=jnp.float32).astype(jnp.bfloat16)
    value_own = jnp.dot(normed_source, w_value, preferred_element_type=jnp.float32).astype(
        jnp.bfloat16
    )
    key_block, value_block = (
        lax.all_gather(key_own, "tp", axis=0, tiled=True),
        lax.all_gather(value_own, "tp", axis=0, tiled=True),
    )
    group_size = tp_size // KVH
    kv_index = lax.axis_index("tp") // group_size
    key_head = lax.dynamic_slice_in_dim(key_block, kv_index * HD, HD, 1)
    value_head = lax.dynamic_slice_in_dim(value_block, kv_index * HD, HD, 1)
    delta = jnp.einsum(
        "rhd,rhd->rh",
        d_attended.reshape(local_rows, -1, HD),
        attended.reshape(local_rows, -1, HD),
        preferred_element_type=jnp.float32,
    ).astype(jnp.bfloat16)
    all_queries = lax.all_gather(query, "sp", axis=0, tiled=True)
    target_total = all_queries.shape[0]
    number = block_count(target_total, 512)
    maxima, totals = lax.map(
        lambda blocked: block_totals(blocked, key_head, scaling),
        all_queries.reshape(number, target_total // number, query_width),
    )
    maxima = maxima.reshape(target_total, -1)
    totals = totals.reshape(target_total, -1)
    maxima, totals = merged((maxima, totals), "sp", merge_totals)
    log_total = maxima + jnp.log(totals)
    block_rows = key_head.shape[0]
    start_state = (
        jnp.zeros((block_rows, HD), jnp.float32),
        jnp.zeros((block_rows, HD), jnp.float32),
    )
    key_acc = start_state[0]
    value_acc = start_state[1]
    cotangent = lax.all_gather(d_attended, "sp", axis=0, tiled=True)
    delta_piece = lax.all_gather(delta, "sp", axis=0, tiled=True)
    row_count = cotangent.shape[0]
    pieces_count = block_count(row_count, 512)
    blocked = tuple(
        (
            member.reshape((pieces_count, row_count // pieces_count) + member.shape[1:])
            for member in (all_queries, cotangent, delta_piece, log_total)
        )
    )

    def fold_inner_step(state, blocks):
        return gradient_block(state, blocks, key_head, value_head, scaling)

    (key_acc, value_acc), grad_rows = lax.scan(fold_inner_step, (key_acc, value_acc), blocked)
    folded = (key_acc, value_acc)
    key_acc = folded[0]
    value_acc = folded[1]
    own_totals = lax.dynamic_slice_in_dim(
        log_total, lax.axis_index("sp") * local_rows, local_rows, 0
    )
    own_queries = query.reshape(local_rows, -1, HD)
    own_grads = d_attended.reshape(local_rows, -1, HD)
    query_start = jnp.zeros((local_rows, query_width // HD, HD), jnp.float32)
    keys_piece = lax.all_gather(key_head, "sp", axis=0, tiled=True)
    values_piece = lax.all_gather(value_head, "sp", axis=0, tiled=True)
    row_count = keys_piece.shape[0]
    pieces_count = block_count(row_count, 512)
    key_blocks = keys_piece.reshape(pieces_count, row_count // pieces_count, HD)
    value_blocks = values_piece.reshape(pieces_count, row_count // pieces_count, HD)

    def key_inner_step(state, blocks):
        keys_now, values_now = blocks
        _, d_scores = score_grads(
            own_queries, own_grads, delta, own_totals, keys_now, values_now, scaling
        )
        return (
            state
            + jnp.einsum("rhs,sd->rhd", d_scores, keys_now, preferred_element_type=jnp.float32)
            * scaling,
            None,
        )

    result, _ = lax.scan(key_inner_step, query_start, (key_blocks, value_blocks))
    d_query = result.reshape(local_rows, query_width).astype(jnp.bfloat16)
    d_w_query = lax.psum_scatter(
        jnp.einsum("rd,rc->dc", normed_target, d_query, preferred_element_type=jnp.float32),
        "sp",
        scatter_dimension=0,
        tiled=True,
    )
    partial_value = jnp.einsum("rc,dc->rd", d_query, w_query, preferred_element_type=jnp.float32)
    d_normed = lax.psum(partial_value.astype(jnp.bfloat16), "tp").astype(jnp.float32)
    d_target = norm_back(target, target_gain, d_normed).astype(jnp.bfloat16)
    stacked = jnp.stack([key_acc, value_acc], axis=1).reshape(tp_size, source_rows, 2 * HD)
    returned = lax.all_to_all(
        stacked.astype(jnp.bfloat16), "tp", split_axis=0, concat_axis=0, tiled=True
    ).astype(stacked.dtype)
    grouped = returned.reshape(KVH, group_size, source_rows, 2, HD).sum(axis=1)
    d_key = (
        grouped[:, :, 0, :].transpose(1, 0, 2).reshape(source_rows, KVH * HD).astype(jnp.bfloat16)
    )
    d_value = (
        grouped[:, :, 1, :].transpose(1, 0, 2).reshape(source_rows, KVH * HD).astype(jnp.bfloat16)
    )
    d_normed_source = jnp.einsum(
        "rc,dc->rd", d_key, w_key, preferred_element_type=jnp.float32
    ) + jnp.einsum("rc,dc->rd", d_value, w_value, preferred_element_type=jnp.float32)
    d_source = norm_back(source, source_gain, d_normed_source)
    return (d_target, d_source, d_w_query)


def solution(mesh):
    return jax.shard_map(
        local,
        mesh=mesh,
        in_specs=(
            P("sp", None),
            P(("sp", "tp"), None),
            P(),
            P(),
            P(None, "tp"),
            P(),
            P(),
            P("sp", "tp"),
            P("sp", "tp"),
        ),
        out_specs=(P("sp", None), P(("sp", "tp"), None), P("sp", "tp")),
        check_vma=False,
    )
```

profile of v0, /device:TPU:0, one launch (start us, length us, event | category | flops | bytes accessed | tf_op | source)
XLA Modules:
  0.0 290.3 jit_solution(17529582570570535842)
XLA Ops:
  7.2 1.4 fusion.48
  8.9 2.2 convolution_convert_fusion.1
  12.0 1.6 convolution_convert_fusion.3
  13.6 6.0 %all_gather.27 = bf16[256,256]{1,0:T(8,128)(2,1)S(1)} all-gather(bf16[128,256]{1,0:T(8,128)(2,1)S(1)} %convolution_convert_fusion.3), channel_id=1, replica_groups=mesh['sp'=16,'tp'=2] {'tp'}, dimensions={0}, use_global_device_ids=true | all-gather | bytes 196608 | tf_op jit(solution)/shard_map/all_gather | solution.py:106
  20.3 1.6 convolution_convert_fusion.2
  21.9 4.9 %all_gather.32 = bf16[256,256]{1,0:T(8,128)(2,1)S(1)} all-gather(bf16[128,256]{1,0:T(8,128)(2,1)S(1)} %convolution_convert_fusion.2), channel_id=1, replica_groups=mesh['sp'=16,'tp'=2] {'tp'}, dimensions={0}, use_global_device_ids=true | all-gather | bytes 196608 | tf_op jit(solution)/shard_map/all_gather | solution.py:107
  30.3 25.2 %all-gather.7.cloned.1.call-done = bf16[2048,512]{1,0:T(8,128)(2,1)} async-done(((bf16[128,512]{1,0:T(8,128)(2,1)}), bf16[2048,512]{1,0:T(8,128)(2,1)}) %all-gather.7.cloned.1.call-update) | async-done | bytes 2097168 | tf_op jit(solution)/shard_map/all_gather | solution.py:119
  55.5 4.2 %copy.78 = bf16[4,512,512]{1,2,0:T(8,128)(2,1)} copy(bf16[4,512,512]{2,1,0:T(8,128)(2,1)} %bitcast.167) | data formatting | bytes 4194304 | tf_op jit(solution)/shard_map/while | solution.py:122
  59.7 7.7 %while.53 = (s32[]{:T(128)}, f32[4,512,4]{1,2,0:T(4,128)S(1)}, f32[4,512,4]{1,2,0:T(4,128)S(1)}, bf16[4,512,512]{1,2,0:T(8,128)(2,1)}, bf16[256,128]{1,0:T(8,128)(2,1)S(1)}, /*index=5*/s32[]{:T(128)}) while((s32[]{:T(128)}, f32[4,512,4]{1,2,0:T(4,128)S(1)}, f32[4,512,4]{1,2,0:T(4,128)S(1)}, bf16[4,512,512]{1,2,0:T(8,128)(2,1)}, ...), condition=%wide.region_5.6_spmd, body=%wide.region_2.5_spmd.sunk | while | flops 136835072 | bytes 5890125 | solution.py:122
  59.7 1.1 constant_dynamic-slice_fusion.9
  61.6 1.1 constant_dynamic-slice_fusion.9
  63.5 1.1 constant_dynamic-slice_fusion.9
  65.5 1.1 constant_dynamic-slice_fusion.9
  67.4 20.9 %all_gather.31 = f32[16,2048,4]{1,2,0:T(4,128)S(1)} all-gather(f32[1,2048,4]{1,2,0:T(4,128)S(1)} %bitcast.179), channel_id=1, replica_groups=mesh['sp'=16,'tp'=2] {'sp'}, dimensions={0}, use_global_device_ids=true | all-gather | bytes 557056 | tf_op jit(solution)/shard_map/all_gather | solution.py:12
  88.3 19.2 %all_gather.30 = f32[16,2048,4]{1,2,0:T(4,128)S(1)} all-gather(f32[1,2048,4]{1,2,0:T(4,128)} %bitcast.178), channel_id=1, replica_groups=mesh['sp'=16,'tp'=2] {'sp'}, dimensions={0}, use_global_device_ids=true | all-gather | bytes 557056 | tf_op jit(solution)/shard_map/all_gather | solution.py:12
  107.5 1.0 while.54
  108.7 25.1 %all-gather.9.cloned.1.call-done = bf16[4096,128]{1,0:T(8,128)(2,1)} async-done(((bf16[256,128]{1,0:T(8,128)(2,1)}), bf16[4096,128]{1,0:T(8,128)(2,1)}) %all-gather.9.cloned.1.call-update) | async-done | bytes 1048592 | tf_op jit(solution)/shard_map/all_gather | solution.py:162
  133.7 24.7 %while.55 = (s32[]{:T(128)}, f32[128,4,128]{2,0,1:T(8,128)S(1)}, bf16[8,512,128]{2,1,0:T(8,128)(2,1)}, bf16[128,4,128]{2,0,1:T(8,128)(2,1)}, f32[128,4]{0,1:T(4,...) while((s32[]{:T(128)}, f32[128,4,128]{2,0,1:T(8,128)S(1)}, ...), condition=%wide.region_9.10_spmd.clone, body=%wide.region_8.9_spmd.clone.sunk | while | flops 202834432 | bytes 3285615 | solution.py:180
  133.7 1.3 convolution_subtract_fusion.2
  135.0 1.8 fusion.104
  136.8 1.3 convolution_subtract_fusion.2
  138.1 1.8 fusion.104
  139.9 1.3 convolution_subtract_fusion.2
  141.2 1.8 fusion.104
  143.0 1.3 convolution_subtract_fusion.2
  144.3 1.8 fusion.104
  146.1 1.3 convolution_subtract_fusion.2
  147.4 1.8 fusion.104
  149.2 1.3 convolution_subtract_fusion.2
  150.5 1.8 fusion.104
  152.3 1.3 convolution_subtract_fusion.2
  153.5 1.8 fusion.104
  155.3 1.3 convolution_subtract_fusion.2
  156.6 1.8 fusion.104
  158.6 1.6 convolution_convert_fusion
  160.3 19.4 %all_gather.35 = bf16[2048,4]{0,1:T(4,128)(2,1)S(1)} all-gather(bf16[128,4]{0,1:T(4,128)(2,1)S(1)} %get-tuple-element.772), channel_id=1, replica_groups=mesh['sp'=16,'tp'=2] {'sp'}, dimensions={0}, use_global_device_ids=true | all-gather | bytes 17408 | tf_op jit(solution)/shard_map/all_gather | solution.py:138
  179.7 2.7 fusion.52
  183.3 42.9 %while.56 = (s32[]{:T(128)}, f32[256,128]{1,0:T(8,128)}, f32[256,128]{1,0:T(8,128)S(1)}, bf16[4,512,512]{1,2,0:T(8,128)(2,1)}, bf16[256,128]{1,0:T(8,128)(2,1)S(...) while((s32[]{:T(128)}, f32[256,128]{1,0:T(8,128)}, ...), condition=%wide.region_13.14_spmd.clone, body=%wide.region_12.13_spmd.clone.sunk | while | flops 541231104 | bytes 14340260 | solution.py:151
  183.3 1.1 constant_dynamic-slice_fusion.10
  184.4 1.9 fusion.112
  186.3 1.1 constant_dynamic-slice_fusion.11
  187.6 3.8 %fusion.113 = f32[256,128]{1,0:T(8,128)} fusion(bf16[512,4,128]{0,2,1:T(8,128)(2,1)} %bitcast.164, f32[512,4,256]{2,0,1:T(8,128)} %fusion.112, bf16[512,4,128]{0,2,1:T(8,128)(2,1)S(1)} %bitcast.161, f32[512,4]{0,1:T(4,128)S(1)} %bitcast_convert_fusion.2, f32[512,4]{0,1:T(4,128)S(1)} %dynamic-slice_bitcast_fusion.2, ...), kind=kOutput, calls=%fused_computation.39.clone.1 | convolution fusion | flops 271155200 | bytes 3489793 | tf_op jit(solution)/shard_map/while/body/eval_jaxpr/rhs,rhd->sd/dot_general | solution.py:83
  191.5 2.4 fusion.114
  193.9 1.1 constant_dynamic-slice_fusion.10
  195.0 1.9 fusion.112
  196.9 1.1 constant_dynamic-slice_fusion.11
  198.3 3.9 %fusion.113 = f32[256,128]{1,0:T(8,128)} fusion(bf16[512,4,128]{0,2,1:T(8,128)(2,1)} %bitcast.164, f32[512,4,256]{2,0,1:T(8,128)} %fusion.112, bf16[512,4,128]{0,2,1:T(8,128)(2,1)S(1)} %bitcast.161, f32[512,4]{0,1:T(4,128)S(1)} %bitcast_convert_fusion.2, f32[512,4]{0,1:T(4,128)S(1)} %dynamic-slice_bitcast_fusion.2, ...), kind=kOutput, calls=%fused_computation.39.clone.1 | convolution fusion | flops 271155200 | bytes 3489793 | tf_op jit(solution)/shard_map/while/body/eval_jaxpr/rhs,rhd->sd/dot_general | solution.py:83
  202.2 2.4 fusion.114
  204.6 1.1 constant_dynamic-slice_fusion.10
  205.7 1.9 fusion.112
  207.6 1.1 constant_dynamic-slice_fusion.11
  208.9 3.9 %fusion.113 = f32[256,128]{1,0:T(8,128)} fusion(bf16[512,4,128]{0,2,1:T(8,128)(2,1)} %bitcast.164, f32[512,4,256]{2,0,1:T(8,128)} %fusion.112, bf16[512,4,128]{0,2,1:T(8,128)(2,1)S(1)} %bitcast.161, f32[512,4]{0,1:T(4,128)S(1)} %bitcast_convert_fusion.2, f32[512,4]{0,1:T(4,128)S(1)} %dynamic-slice_bitcast_fusion.2, ...), kind=kOutput, calls=%fused_computation.39.clone.1 | convolution fusion | flops 271155200 | bytes 3489793 | tf_op jit(solution)/shard_map/while/body/eval_jaxpr/rhs,rhd->sd/dot_general | solution.py:83
  212.8 2.4 fusion.114
  215.3 1.1 constant_dynamic-slice_fusion.10
  216.4 1.9 fusion.112
  218.3 1.1 constant_dynamic-slice_fusion.11
  219.7 4.0 %fusion.113 = f32[256,128]{1,0:T(8,128)} fusion(bf16[512,4,128]{0,2,1:T(8,128)(2,1)} %bitcast.164, f32[512,4,256]{2,0,1:T(8,128)} %fusion.112, bf16[512,4,128]{0,2,1:T(8,128)(2,1)S(1)} %bitcast.161, f32[512,4]{0,1:T(4,128)S(1)} %bitcast_convert_fusion.2, f32[512,4]{0,1:T(4,128)S(1)} %dynamic-slice_bitcast_fusion.2, ...), kind=kOutput, calls=%fused_computation.39.clone.1 | convolution fusion | flops 271155200 | bytes 3489793 | tf_op jit(solution)/shard_map/while/body/eval_jaxpr/rhs,rhd->sd/dot_general | solution.py:83
  223.7 2.5 fusion.114
  227.5 6.9 %all_to_all.5 = bf16[2,128,256]{2,1,0:T(8,128)(2,1)S(1)} all-to-all(bf16[2,128,256]{2,1,0:T(8,128)(2,1)S(1)} %convert_element_type.103), channel_id=1, replica_groups=mesh['sp'=16,'tp'=2] {'tp'}, dimensions={0} | all-to-all | bytes 262144 | tf_op jit(solution)/shard_map/all_to_all | solution.py:192
  234.9 1.8 fusion.60
  237.4 1.2 add_add_fusion
  238.6 1.3 fusion.51
  239.9 2.2 fusion.43
  242.1 41.4 %reduce-scatter.2.cloned.1.call-done = f32[128,512]{1,0:T(8,128)} async-done(((f32[2048,512]{1,0:T(8,128)}), f32[128,512]{1,0:T(8,128)}) %reduce-scatter.2.cloned.1.call-update) | async-done | bytes 262160 | tf_op jit(solution)/shard_map/reduce_scatter | solution.py:182
  (143 shorter events, 13.7 us)
Async XLA Ops:
  7.2 1.8 copy-start
  7.2 4.0 %copy-start.5 = (bf16[128,2048]{1,0:T(8,128)(2,1)S(1)}, bf16[128,2048]{1,0:T(8,128)(2,1)}, u32[]{:S(2)}) copy-start(bf16[128,2048]{1,0:T(8,128)(2,1)} %param.18) | copy-start | bytes 1572868
  7.2 4.8 %copy-start.14 = (f32[2048]{0:T(1024)S(1)}, f32[2048]{0:T(1024)}, u32[]{:S(2)}) copy-start(f32[2048]{0:T(1024)} %param.20) | copy-start | bytes 24580
  7.2 48.3 %all-gather.7.cloned.1.call-start = ((), (), s32[]{:S(2)}) async-start(), calls=%async_computation.3 | async-start | bytes 2228224 | tf_op jit(solution)/shard_map/all_gather | solution.py:119
  8.6 2.8 copy-start.15
  11.1 97.5 %all-gather.5.cloned.1.call-start = ((), (), s32[]{:S(2)}) async-start(), calls=%async_computation.2 | async-start | bytes 1114112 | tf_op jit(solution)/shard_map/all_gather | solution.py:161
  11.4 0.5 copy-start.19
  11.9 14.9 %copy-start.17 = (f32[128]{0:T(128)}, f32[128]{0:T(128)S(1)}, u32[]{:S(2)}) copy-start(f32[128]{0:T(128)S(1)} %fusion.57) | copy-start | bytes 1540
  11.9 16.2 %copy-start.8 = (bf16[128,512]{1,0:T(8,128)(2,1)S(1)}, bf16[128,512]{1,0:T(8,128)(2,1)}, u32[]{:S(2)}) copy-start(bf16[128,512]{1,0:T(8,128)(2,1)} %param.25) | copy-start | bytes 393220
  12.0 16.3 %copy-start.9 = (bf16[128,512]{1,0:T(8,128)(2,1)S(1)}, bf16[128,512]{1,0:T(8,128)(2,1)}, u32[]{:S(2)}) copy-start(bf16[128,512]{1,0:T(8,128)(2,1)} %convolution_convert_fusion.1) | copy-start | bytes 393220
  13.6 16.3 %copy-start.11 = (bf16[128,512]{1,0:T(8,128)(2,1)S(1)}, bf16[128,512]{1,0:T(8,128)(2,1)}, u32[]{:S(2)}) copy-start(bf16[128,512]{1,0:T(8,128)(2,1)} %param.24) | copy-start | bytes 393220
  20.3 113.5 %all-gather.9.cloned.1.call-start = ((), (), s32[]{:S(2)}) async-start(), calls=%async_computation.4 | async-start | bytes 1114112 | tf_op jit(solution)/shard_map/all_gather | solution.py:162
  27.5 155.0 %all-gather.11.cloned.1.call-start = ((), (), s32[]{:S(2)}) async-start(), calls=%async_computation.6 | async-start | bytes 2228224 | tf_op jit(solution)/shard_map/all_gather | solution.py:137
  28.1 210.5 %all-reduce.2.cloned.1.call-start = ((), (), s32[]{:S(2)}) async-start(), calls=%async_computation.5 | async-start | bytes 1048576 | tf_op jit(solution)/shard_map/psum | solution.py:189
  55.5 4.2 %copy-start.2 = (bf16[256,128]{1,0:T(8,128)(2,1)S(1)}, bf16[256,128]{1,0:T(8,128)(2,1)}, u32[]{:S(2)}) copy-start(bf16[256,128]{1,0:T(8,128)(2,1)} %constant_dynamic-slice_fusion.5) | copy-start | bytes 196612
  67.4 20.9 %copy-start.13 = (f32[4,512,4]{1,2,0:T(4,128)}, f32[4,512,4]{1,2,0:T(4,128)S(1)}, u32[]{:S(2)}) copy-start(f32[4,512,4]{1,2,0:T(4,128)S(1)} %get-tuple-element.254) | copy-start | bytes 98308
  158.4 21.3 %copy-start.3 = (bf16[128,2048]{1,0:T(8,128)(2,1)S(1)}, bf16[128,2048]{1,0:T(8,128)(2,1)}, u32[]{:S(2)}) copy-start(bf16[128,2048]{1,0:T(8,128)(2,1)} %param.17) | copy-start | bytes 1572868
  158.4 21.3 %copy-start.12 = (f32[2048]{0:T(1024)S(1)}, f32[2048]{0:T(1024)}, u32[]{:S(2)}) copy-start(f32[2048]{0:T(1024)} %param.19) | copy-start | bytes 24580
  160.2 123.3 %reduce-scatter.2.cloned.1.call-start = ((), (), s32[]{:S(2)}) async-start(), calls=%async_computation.7 | async-start | bytes 4456448 | tf_op jit(solution)/shard_map/reduce_scatter | solution.py:182
  182.5 0.9 copy-start.10
  184.4 1.9 copy-start.1
  195.0 1.9 copy-start.1
  205.7 1.9 copy-start.1
  216.4 1.9 copy-start.1
  227.2 9.5 %copy-start.6 = (bf16[128,2048]{1,0:T(8,128)(2,1)S(1)}, bf16[128,2048]{1,0:T(8,128)(2,1)}, u32[]{:S(2)}) copy-start(bf16[128,2048]{1,0:T(8,128)(2,1)} %param.18) | copy-start | bytes 1572868
  234.9 1.8 copy-start.7
  236.7 0.6 copy-start.20
  236.7 0.7 copy-start.18
  237.3 1.3 copy-start.4
  237.3 2.6 copy-start.16
Sparse Core Ops, SparseCore 0:
  11.3 44.1 all-gather.6
  57.6 36.9 all-gather.4
  96.8 36.9 all-gather.8
  135.7 40.4 all-gather.10
  178.9 27.3 all-reduce.1
  210.6 72.8 reduce-scatter.1
where the time goes:
time: 292 us; the launch traced here: 290 us
  waiting for transfers between devices  92.4 us (32%)
  blocking collectives  77.4 us (27%)
  matrix products  71.2 us (24%)
  local copies, waits for them, and re-layouts  23.9 us (8%)
  between operations  14.5 us (5%)
  other arithmetic  9.92 us (3%)
    reduce_scatter x1, waiting for transfers between devices, local(): lax.psum_scatter(jnp.einsum('rd,rc->dc', normed_target, d_query, preferre...  41.4 us
    all_gather x2, blocking collectives, merged(): everything = jax.tree.map(lambda part: lax.all_gather(part, axis), shard)  40.1 us
    all_gather x1, waiting for transfers between devices, local(): all_queries = lax.all_gather(query, 'sp', axis=0, tiled=True)  25.2 us
    all_gather x1, waiting for transfers between devices, local(): values_piece = lax.all_gather(value_head, 'sp', axis=0, tiled=True)  25.1 us
    all_gather x1, blocking collectives, local(): delta_piece = lax.all_gather(delta, 'sp', axis=0, tiled=True)  19.4 us
    dot_general x4, matrix products, gradient_block(): jnp.einsum('rhs,rhd->sd', d_scores, query_heads, preferred_element_type=j...  15.7 us
    dot_general x8, matrix products, key_inner_step(): jnp.einsum('rhs,sd->rhd', d_scores, keys_now, preferred_element_type=jnp....  14.2 us
    dynamic_slice x16, local copies, waits for them, and re-layouts, local(): lax.map(lambda blocked: block_totals(blocked, key_head, scaling), all_que...  13.9 us
  transfers between devices with their start and end apart: 6, of which 3 were waited for; matrix products, arithmetic and copies ran while one was open for 34% of the time, Pallas kernels for 0%

commit v1 on v0

--- a/solution.py
+++ b/solution.py
@@ -159,7 +159,12 @@
     own_grads = d_attended.reshape(local_rows, -1, HD)
     query_start = jnp.zeros((local_rows, query_width // HD, HD), jnp.float32)
     keys_piece = lax.all_gather(key_head, "sp", axis=0, tiled=True)
-    values_piece = lax.all_gather(value_head, "sp", axis=0, tiled=True)
+    ring = [value_head]
+    for hop in range(15):
+        ring.append(lax.ppermute(ring[-1], "sp", [(dev, (dev + 1) % 16) for dev in range(16)]))
+    values_piece = jnp.roll(
+        jnp.concatenate(ring[::-1], axis=0), (lax.axis_index("sp") + 1) * ring[0].shape[0], axis=0
+    )
     row_count = keys_piece.shape[0]
     pieces_count = block_count(row_count, 512)
     key_blocks = keys_piece.reshape(pieces_count, row_count // pieces_count, HD)

time: 292 us -> 326 us (1.12)
  waiting for transfers between devices: 92.4 us -> 124 us
  local copies, waits for them, and re-layouts: 23.9 us -> 31.2 us
    ppermute x0 -> x15, waiting for transfers between devices: none -> 96.6 us  [local(): lax.ppermute(ring[-1], 'sp', [(dev, (dev + 1) % 16) for dev in range(16)])]
    all_gather x1, waiting for transfers between devices: 25.2 us -> 0.01 us  [local(): all_queries = lax.all_gather(query, 'sp', axis=0, tiled=True)]
    all_gather x1 -> x0, waiting for transfers between devices: 25.1 us -> none  [local(): values_piece = lax.all_gather(value_head, 'sp', axis=0, tiled=True)]
    reduce_scatter x1, waiting for transfers between devices: 41.4 us -> 27.2 us  [local(): lax.psum_scatter(jnp.einsum('rd,rc->dc', normed_target, d_query, preferre...]
    unnamed x44 -> x79, local copies, waits for them, and re-layouts: 3.42 us -> 8.67 us
  transfers between devices with their start and end apart: 6 -> 20, of which waited for: 3 -> 16; matrix products, arithmetic and copies ran while one was open for 34% -> 32% of each run, Pallas kernels for 0% -> 0%
where the time goes in v1:
time: 326 us; the launch traced here: 324 us
  waiting for transfers between devices  124 us (38%)
  blocking collectives  75.1 us (23%)
  matrix products  68.9 us (21%)
  local copies, waits for them, and re-layouts  31.2 us (10%)
  between operations  14.3 us (4%)
  other arithmetic  9.59 us (3%)
    ppermute x15, waiting for transfers between devices, local(): lax.ppermute(ring[-1], 'sp', [(dev, (dev + 1) % 16) for dev in range(16)])  96.6 us
    all_gather x2, blocking collectives, merged(): everything = jax.tree.map(lambda part: lax.all_gather(part, axis), shard)  39.6 us
    reduce_scatter x1, waiting for transfers between devices, local(): lax.psum_scatter(jnp.einsum('rd,rc->dc', normed_target, d_query, preferre...  27.2 us
    all_gather x1, blocking collectives, local(): delta_piece = lax.all_gather(delta, 'sp', axis=0, tiled=True)  17.5 us
    dot_general x8, matrix products, key_inner_step(): jnp.einsum('rhs,sd->rhd', d_scores, keys_now, preferred_element_type=jnp....  14.2 us
    dynamic_slice x16, local copies, waits for them, and re-layouts, local(): lax.map(lambda blocked: block_totals(blocked, key_head, scaling), all_que...  13.9 us
    dot_general x4, matrix products, gradient_block(): jnp.einsum('rhs,rhd->sd', d_scores, query_heads, preferred_element_type=j...  13.2 us
    dot_general x8, matrix products, score_grads(): jnp.einsum('rhd,sd->rhs', grad_heads, value_head, preferred_element_type=...  10.1 us
  transfers between devices with their start and end apart: 20, of which 16 were waited for; matrix products, arithmetic and copies ran while one was open for 32% of the time, Pallas kernels for 0%

profile of v1, /device:TPU:0, one launch (start us, length us, event | category | flops | bytes accessed | tf_op | source)
XLA Modules:
  0.0 324.2 jit_solution(10792523218728184396)
XLA Ops:
  7.2 1.4 fusion.48
  8.9 2.2 convolution_convert_fusion.1
  11.9 1.6 convolution_convert_fusion.3
  13.6 5.9 %all_gather.24 = bf16[256,256]{1,0:T(8,128)(2,1)S(1)} all-gather(bf16[128,256]{1,0:T(8,128)(2,1)S(1)} %convolution_convert_fusion.3), channel_id=1, replica_groups=mesh['sp'=16,'tp'=2] {'tp'}, dimensions={0}, use_global_device_ids=true | all-gather | bytes 196608 | tf_op jit(solution)/shard_map/all_gather | solution.py:106
  20.1 1.6 convolution_convert_fusion.2
  21.7 4.9 %all_gather.29 = bf16[256,256]{1,0:T(8,128)(2,1)S(1)} all-gather(bf16[128,256]{1,0:T(8,128)(2,1)S(1)} %convolution_convert_fusion.2), channel_id=1, replica_groups=mesh['sp'=16,'tp'=2] {'tp'}, dimensions={0}, use_global_device_ids=true | all-gather | bytes 196608 | tf_op jit(solution)/shard_map/all_gather | solution.py:107
  26.7 7.1 %collective-permute-done = bf16[256,128]{1,0:T(8,128)(2,1)S(1)} collective-permute-done((bf16[256,128]{1,0:T(8,128)(2,1)S(1)}, bf16[256,128]{1,0:T(8,128)(2,1)S(1)}, u32[]{:S(2)}, u32[]{:S(2)}) %collective-permute-start) | collective-permute-done | bytes 65568 | tf_op jit(solution)/shard_map/ppermute | solution.py:164
  33.8 6.4 %collective-permute-done.1 = bf16[256,128]{1,0:T(8,128)(2,1)S(1)} collective-permute-done((bf16[256,128]{1,0:T(8,128)(2,1)S(1)}, bf16[256,128]{1,0:T(8,128)(2,1)S(1)}, u32[]{:S(2)}, u32[]{:S(2)}) %collective-permute-start.1) | collective-permute-done | bytes 65568 | tf_op jit(solution)/shard_map/ppermute | solution.py:164
  40.2 7.9 %collective-permute-done.2 = bf16[256,128]{1,0:T(8,128)(2,1)S(1)} collective-permute-done((bf16[256,128]{1,0:T(8,128)(2,1)S(1)}, bf16[256,128]{1,0:T(8,128)(2,1)S(1)}, u32[]{:S(2)}, u32[]{:S(2)}) %collective-permute-start.2) | collective-permute-done | bytes 65568 | tf_op jit(solution)/shard_map/ppermute | solution.py:164
  48.1 7.1 %collective-permute-done.3 = bf16[256,128]{1,0:T(8,128)(2,1)S(1)} collective-permute-done((bf16[256,128]{1,0:T(8,128)(2,1)S(1)}, bf16[256,128]{1,0:T(8,128)(2,1)S(1)}, u32[]{:S(2)}, u32[]{:S(2)}) %collective-permute-start.3) | collective-permute-done | bytes 65568 | tf_op jit(solution)/shard_map/ppermute | solution.py:164
  55.2 6.4 %collective-permute-done.4 = bf16[256,128]{1,0:T(8,128)(2,1)S(1)} collective-permute-done((bf16[256,128]{1,0:T(8,128)(2,1)S(1)}, bf16[256,128]{1,0:T(8,128)(2,1)S(1)}, u32[]{:S(2)}, u32[]{:S(2)}) %collective-permute-start.4) | collective-permute-done | bytes 65568 | tf_op jit(solution)/shard_map/ppermute | solution.py:164
  61.6 6.4 %collective-permute-done.5 = bf16[256,128]{1,0:T(8,128)(2,1)S(1)} collective-permute-done((bf16[256,128]{1,0:T(8,128)(2,1)S(1)}, bf16[256,128]{1,0:T(8,128)(2,1)S(1)}, u32[]{:S(2)}, u32[]{:S(2)}) %collective-permute-start.5) | collective-permute-done | bytes 65568 | tf_op jit(solution)/shard_map/ppermute | solution.py:164
  68.0 6.6 %collective-permute-done.6 = bf16[256,128]{1,0:T(8,128)(2,1)S(1)} collective-permute-done((bf16[256,128]{1,0:T(8,128)(2,1)S(1)}, bf16[256,128]{1,0:T(8,128)(2,1)S(1)}, u32[]{:S(2)}, u32[]{:S(2)}) %collective-permute-start.6) | collective-permute-done | bytes 65568 | tf_op jit(solution)/shard_map/ppermute | solution.py:164
  74.7 6.4 %collective-permute-done.7 = bf16[256,128]{1,0:T(8,128)(2,1)S(1)} collective-permute-done((bf16[256,128]{1,0:T(8,128)(2,1)S(1)}, bf16[256,128]{1,0:T(8,128)(2,1)S(1)}, u32[]{:S(2)}, u32[]{:S(2)}) %collective-permute-start.7) | collective-permute-done | bytes 65568 | tf_op jit(solution)/shard_map/ppermute | solution.py:164
  81.0 7.3 %collective-permute-done.8 = bf16[256,128]{1,0:T(8,128)(2,1)S(1)} collective-permute-done((bf16[256,128]{1,0:T(8,128)(2,1)S(1)}, bf16[256,128]{1,0:T(8,128)(2,1)S(1)}, u32[]{:S(2)}, u32[]{:S(2)}) %collective-permute-start.8) | collective-permute-done | bytes 65568 | tf_op jit(solution)/shard_map/ppermute | solution.py:164
  88.3 6.7 %collective-permute-done.9 = bf16[256,128]{1,0:T(8,128)(2,1)S(1)} collective-permute-done((bf16[256,128]{1,0:T(8,128)(2,1)S(1)}, bf16[256,128]{1,0:T(8,128)(2,1)S(1)}, u32[]{:S(2)}, u32[]{:S(2)}) %collective-permute-start.9) | collective-permute-done | bytes 65568 | tf_op jit(solution)/shard_map/ppermute | solution.py:164
  95.1 6.4 %collective-permute-done.10 = bf16[256,128]{1,0:T(8,128)(2,1)S(1)} collective-permute-done((bf16[256,128]{1,0:T(8,128)(2,1)S(1)}, bf16[256,128]{1,0:T(8,128)(2,1)S(1)}, u32[]{:S(2)}, u32[]{:S(2)}) %collective-permute-start.10) | collective-permute-done | bytes 65568 | tf_op jit(solution)/shard_map/ppermute | solution.py:164
  102.1 6.4 %collective-permute-done.11 = bf16[256,128]{1,0:T(8,128)(2,1)S(1)} collective-permute-done((bf16[256,128]{1,0:T(8,128)(2,1)S(1)}, bf16[256,128]{1,0:T(8,128)(2,1)S(1)}, u32[]{:S(2)}, u32[]{:S(2)}) %collective-permute-start.11) | collective-permute-done | bytes 65568 | tf_op jit(solution)/shard_map/ppermute | solution.py:164
  108.6 6.4 %collective-permute-done.12 = bf16[256,128]{1,0:T(8,128)(2,1)} collective-permute-done((bf16[256,128]{1,0:T(8,128)(2,1)S(1)}, bf16[256,128]{1,0:T(8,128)(2,1)}, u32[]{:S(2)}, u32[]{:S(2)}) %collective-permute-start.12) | collective-permute-done | bytes 65568 | tf_op jit(solution)/shard_map/ppermute | solution.py:164
  116.9 4.9 %collective-permute-done.13 = bf16[256,128]{1,0:T(8,128)(2,1)} collective-permute-done((bf16[256,128]{1,0:T(8,128)(2,1)}, bf16[256,128]{1,0:T(8,128)(2,1)}, u32[]{:S(2)}, u32[]{:S(2)}) %collective-permute-start.13) | collective-permute-done | bytes 65568 | tf_op jit(solution)/shard_map/ppermute | solution.py:164
  124.3 4.2 %collective-permute-done.14 = bf16[256,128]{1,0:T(8,128)(2,1)} collective-permute-done((bf16[256,128]{1,0:T(8,128)(2,1)}, bf16[256,128]{1,0:T(8,128)(2,1)}, u32[]{:S(2)}, u32[]{:S(2)}) %collective-permute-start.14) | collective-permute-done | bytes 65568 | tf_op jit(solution)/shard_map/ppermute | solution.py:164
  135.2 4.2 %copy.78 = bf16[4,512,512]{1,2,0:T(8,128)(2,1)} copy(bf16[4,512,512]{2,1,0:T(8,128)(2,1)} %bitcast.168) | data formatting | bytes 4194304 | tf_op jit(solution)/shard_map/while | solution.py:122
  139.4 7.7 %while.53 = (s32[]{:T(128)}, f32[4,512,4]{1,2,0:T(4,128)S(1)}, f32[4,512,4]{1,2,0:T(4,128)S(1)}, bf16[4,512,512]{1,2,0:T(8,128)(2,1)}, bf16[256,128]{1,0:T(8,128)(2,1)S(1)}, /*index=5*/s32[]{:T(128)}) while((s32[]{:T(128)}, f32[4,512,4]{1,2,0:T(4,128)S(1)}, f32[4,512,4]{1,2,0:T(4,128)S(1)}, bf16[4,512,512]{1,2,0:T(8,128)(2,1)}, ...), condition=%wide.region_5.6_spmd, body=%wide.region_2.5_spmd.sunk | while | flops 136835072 | bytes 5890125 | solution.py:122
  147.1 18.7 %all_gather.28 = f32[16,2048,4]{1,2,0:T(4,128)S(1)} all-gather(f32[1,2048,4]{1,2,0:T(4,128)S(1)} %bitcast.179), channel_id=1, replica_groups=mesh['sp'=16,'tp'=2] {'sp'}, dimensions={0}, use_global_device_ids=true | all-gather | bytes 557056 | tf_op jit(solution)/shard_map/all_gather | solution.py:12
  165.8 20.9 %all_gather.27 = f32[16,2048,4]{1,2,0:T(4,128)S(1)} all-gather(f32[1,2048,4]{1,2,0:T(4,128)S(1)} %bitcast.178), channel_id=1, replica_groups=mesh['sp'=16,'tp'=2] {'sp'}, dimensions={0}, use_global_device_ids=true | all-gather | bytes 557056 | tf_op jit(solution)/shard_map/all_gather | solution.py:12
  187.9 24.7 %while.55 = (s32[]{:T(128)}, f32[128,4,128]{2,0,1:T(8,128)S(1)}, bf16[8,512,128]{2,1,0:T(8,128)(2,1)}, bf16[128,4,128]{2,0,1:T(8,128)(2,1)}, f32[128,4]{0,1:T(4,...) while((s32[]{:T(128)}, f32[128,4,128]{2,0,1:T(8,128)S(1)}, ...), condition=%wide.region_9.10_spmd.clone, body=%wide.region_8.9_spmd.clone.sunk | while | flops 202834432 | bytes 3285615 | solution.py:185
  187.9 1.3 convolution_subtract_fusion.2
  189.2 1.8 fusion.104
  191.0 1.3 convolution_subtract_fusion.2
  192.3 1.8 fusion.104
  194.1 1.3 convolution_subtract_fusion.2
  195.3 1.8 fusion.104
  197.1 1.3 convolution_subtract_fusion.2
  198.4 1.8 fusion.104
  200.2 1.3 convolution_subtract_fusion.2
  201.5 1.8 fusion.104
  203.3 1.3 convolution_subtract_fusion.2
  204.6 1.8 fusion.104
  206.4 1.3 convolution_subtract_fusion.2
  207.7 1.8 fusion.104
  209.5 1.3 convolution_subtract_fusion.2
  210.7 1.8 fusion.104
  212.7 1.6 convolution_convert_fusion
  214.4 17.5 %all_gather.31 = bf16[2048,4]{0,1:T(4,128)(2,1)S(1)} all-gather(bf16[128,4]{0,1:T(4,128)(2,1)S(1)} %get-tuple-element.793), channel_id=1, replica_groups=mesh['sp'=16,'tp'=2] {'sp'}, dimensions={0}, use_global_device_ids=true | all-gather | bytes 17408 | tf_op jit(solution)/shard_map/all_gather | solution.py:138
  231.9 2.8 fusion.52
  234.7 40.6 %while.56 = (s32[]{:T(128)}, f32[256,128]{1,0:T(8,128)S(1)}, f32[256,128]{1,0:T(8,128)S(1)}, bf16[4,512,512]{1,2,0:T(8,128)(2,1)}, bf16[256,128]{1,0:T(8,128)(2,...) while((s32[]{:T(128)}, f32[256,128]{1,0:T(8,128)S(1)}, ...), condition=%wide.region_13.14_spmd.clone, body=%wide.region_12.13_spmd.clone.sunk | while | flops 541231104 | bytes 14340260 | solution.py:151
  235.8 1.9 fusion.112
  239.0 3.2 fusion.113
  242.3 2.4 fusion.114
  245.8 1.9 fusion.112
  249.0 3.4 %fusion.113 = f32[256,128]{1,0:T(8,128)S(1)} fusion(bf16[512,4,128]{0,2,1:T(8,128)(2,1)} %bitcast.164, f32[512,4,256]{2,0,1:T(8,128)} %fusion.112, bf16[512,4,128]{0,2,1:T(8,128)(2,1)S(1)} %bitcast.161, f32[512,4]{0,1:T(4,128)S(1)} %bitcast_convert_fusion.2, f32[512,4]{0,1:T(4,128)S(1)} %dynamic-slice_bitcast_fusion.2, ...), kind=kOutput, calls=%fused_computation.39.clone.1 | convolution fusion | flops 271155200 | bytes 3489793 | tf_op jit(solution)/shard_map/while/body/eval_jaxpr/rhs,rhd->sd/dot_general | solution.py:83
  252.4 2.5 fusion.114
  256.1 1.9 fusion.112
  259.3 3.4 %fusion.113 = f32[256,128]{1,0:T(8,128)S(1)} fusion(bf16[512,4,128]{0,2,1:T(8,128)(2,1)} %bitcast.164, f32[512,4,256]{2,0,1:T(8,128)} %fusion.112, bf16[512,4,128]{0,2,1:T(8,128)(2,1)S(1)} %bitcast.161, f32[512,4]{0,1:T(4,128)S(1)} %bitcast_convert_fusion.2, f32[512,4]{0,1:T(4,128)S(1)} %dynamic-slice_bitcast_fusion.2, ...), kind=kOutput, calls=%fused_computation.39.clone.1 | convolution fusion | flops 271155200 | bytes 3489793 | tf_op jit(solution)/shard_map/while/body/eval_jaxpr/rhs,rhd->sd/dot_general | solution.py:83
  262.7 2.6 fusion.114
  266.4 1.9 fusion.112
  269.6 3.2 fusion.113
  272.8 2.5 fusion.114
  275.6 7.1 %all_to_all.5 = bf16[2,128,256]{2,1,0:T(8,128)(2,1)S(1)} all-to-all(bf16[2,128,256]{2,1,0:T(8,128)(2,1)S(1)} %convert_element_type.103), channel_id=1, replica_groups=mesh['sp'=16,'tp'=2] {'tp'}, dimensions={0} | all-to-all | bytes 262144 | tf_op jit(solution)/shard_map/all_to_all | solution.py:197
  283.3 1.8 fusion.60
  285.8 1.2 add_add_fusion
  287.0 1.3 fusion.51
  288.3 2.1 fusion.43
  290.5 27.2 %reduce-scatter.2.cloned.1.call-done = f32[128,512]{1,0:T(8,128)} async-done(((f32[2048,512]{1,0:T(8,128)}), f32[128,512]{1,0:T(8,128)}) %reduce-scatter.2.cloned.1.call-update) | async-done | bytes 262160 | tf_op jit(solution)/shard_map/reduce_scatter | solution.py:187
  (207 shorter events, 34.3 us)
Async XLA Ops:
  7.2 1.8 copy-start
  7.2 4.0 %copy-start.5 = (bf16[128,2048]{1,0:T(8,128)(2,1)S(1)}, bf16[128,2048]{1,0:T(8,128)(2,1)}, u32[]{:S(2)}) copy-start(bf16[128,2048]{1,0:T(8,128)(2,1)} %param.18) | copy-start | bytes 1572868
  7.2 4.7 %copy-start.16 = (f32[2048]{0:T(1024)S(1)}, f32[2048]{0:T(1024)}, u32[]{:S(2)}) copy-start(f32[2048]{0:T(1024)} %param.20) | copy-start | bytes 24580
  7.2 128.0 %all-gather.6.cloned.1.call-start = ((), (), s32[]{:S(2)}) async-start(), calls=%async_computation.3 | async-start | bytes 2228224 | tf_op jit(solution)/shard_map/all_gather | solution.py:119
  8.6 2.8 copy-start.17
  11.1 176.7 %all-gather.4.cloned.1.call-start = ((), (), s32[]{:S(2)}) async-start(), calls=%async_computation.2 | async-start | bytes 1114112 | tf_op jit(solution)/shard_map/all_gather | solution.py:161
  11.4 0.5 copy-start.21
  11.9 14.7 %copy-start.19 = (f32[128]{0:T(128)}, f32[128]{0:T(128)S(1)}, u32[]{:S(2)}) copy-start(f32[128]{0:T(128)S(1)} %fusion.57) | copy-start | bytes 1540
  11.9 103.1 %copy-start.9 = (bf16[128,512]{1,0:T(8,128)(2,1)S(1)}, bf16[128,512]{1,0:T(8,128)(2,1)}, u32[]{:S(2)}) copy-start(bf16[128,512]{1,0:T(8,128)(2,1)} %convolution_convert_fusion.1) | copy-start | bytes 393220
  11.9 103.7 %copy-start.8 = (bf16[128,512]{1,0:T(8,128)(2,1)S(1)}, bf16[128,512]{1,0:T(8,128)(2,1)}, u32[]{:S(2)}) copy-start(bf16[128,512]{1,0:T(8,128)(2,1)} %param.25) | copy-start | bytes 393220
  20.1 214.6 %all-gather.8.cloned.1.call-start = ((), (), s32[]{:S(2)}) async-start(), calls=%async_computation.5 | async-start | bytes 2228224 | tf_op jit(solution)/shard_map/all_gather | solution.py:137
  26.7 81.8 %copy-start.15 = (bf16[256,128]{1,0:T(8,128)(2,1)}, bf16[256,128]{1,0:T(8,128)(2,1)S(1)}, u32[]{:S(2)}) copy-start(bf16[256,128]{1,0:T(8,128)(2,1)S(1)} %constant_dynamic-slice_fusion.4) | copy-start | bytes 196612
  26.7 7.1 %collective-permute-start = (bf16[256,128]{1,0:T(8,128)(2,1)S(1)}, bf16[256,128]{1,0:T(8,128)(2,1)S(1)}, u32[]{:S(2)}, u32[]{:S(2)}) collective-permute-start(bf16[256,128]{1,0:T(8,128)(2,1)S(1)} %constant_dynamic-slice_fusion.4), channel_id=1, source_target_pairs={{0,2},{2,4},{4,6},{6,8},{8,10},{10,12},{12,14},{14,16},{16,18},{18... | collective-permute-start | bytes 196616 | tf_op jit(solution)/shard_map/ppermute | solution.py:164
  33.8 6.4 %collective-permute-start.1 = (bf16[256,128]{1,0:T(8,128)(2,1)S(1)}, bf16[256,128]{1,0:T(8,128)(2,1)S(1)}, u32[]{:S(2)}, u32[]{:S(2)}) collective-permute-start(bf16[256,128]{1,0:T(8,128)(2,1)S(1)} %collective-permute-done), channel_id=1, source_target_pairs={{0,2},{2,4},{4,6},{6,8},{8,10},{10,12},{12,14},{14,16},{16,18},{18... | collective-permute-start | bytes 196616 | tf_op jit(solution)/shard_map/ppermute | solution.py:164
  40.2 7.9 %collective-permute-start.2 = (bf16[256,128]{1,0:T(8,128)(2,1)S(1)}, bf16[256,128]{1,0:T(8,128)(2,1)S(1)}, u32[]{:S(2)}, u32[]{:S(2)}) collective-permute-start(bf16[256,128]{1,0:T(8,128)(2,1)S(1)} %collective-permute-done.1), channel_id=1, source_target_pairs={{0,2},{2,4},{4,6},{6,8},{8,10},{10,12},{12,14},{14,16},{16,18},{18... | collective-permute-start | bytes 196616 | tf_op jit(solution)/shard_map/ppermute | solution.py:164
  48.1 7.1 %collective-permute-start.3 = (bf16[256,128]{1,0:T(8,128)(2,1)S(1)}, bf16[256,128]{1,0:T(8,128)(2,1)S(1)}, u32[]{:S(2)}, u32[]{:S(2)}) collective-permute-start(bf16[256,128]{1,0:T(8,128)(2,1)S(1)} %collective-permute-done.2), channel_id=1, source_target_pairs={{0,2},{2,4},{4,6},{6,8},{8,10},{10,12},{12,14},{14,16},{16,18},{18... | collective-permute-start | bytes 196616 | tf_op jit(solution)/shard_map/ppermute | solution.py:164
  55.2 6.4 %collective-permute-start.4 = (bf16[256,128]{1,0:T(8,128)(2,1)S(1)}, bf16[256,128]{1,0:T(8,128)(2,1)S(1)}, u32[]{:S(2)}, u32[]{:S(2)}) collective-permute-start(bf16[256,128]{1,0:T(8,128)(2,1)S(1)} %collective-permute-done.3), channel_id=1, source_target_pairs={{0,2},{2,4},{4,6},{6,8},{8,10},{10,12},{12,14},{14,16},{16,18},{18... | collective-permute-start | bytes 196616 | tf_op jit(solution)/shard_map/ppermute | solution.py:164
  61.6 6.4 %collective-permute-start.5 = (bf16[256,128]{1,0:T(8,128)(2,1)S(1)}, bf16[256,128]{1,0:T(8,128)(2,1)S(1)}, u32[]{:S(2)}, u32[]{:S(2)}) collective-permute-start(bf16[256,128]{1,0:T(8,128)(2,1)S(1)} %collective-permute-done.4), channel_id=1, source_target_pairs={{0,2},{2,4},{4,6},{6,8},{8,10},{10,12},{12,14},{14,16},{16,18},{18... | collective-permute-start | bytes 196616 | tf_op jit(solution)/shard_map/ppermute | solution.py:164
  68.0 6.6 %collective-permute-start.6 = (bf16[256,128]{1,0:T(8,128)(2,1)S(1)}, bf16[256,128]{1,0:T(8,128)(2,1)S(1)}, u32[]{:S(2)}, u32[]{:S(2)}) collective-permute-start(bf16[256,128]{1,0:T(8,128)(2,1)S(1)} %collective-permute-done.5), channel_id=1, source_target_pairs={{0,2},{2,4},{4,6},{6,8},{8,10},{10,12},{12,14},{14,16},{16,18},{18... | collective-permute-start | bytes 196616 | tf_op jit(solution)/shard_map/ppermute | solution.py:164
  74.6 6.4 %collective-permute-start.7 = (bf16[256,128]{1,0:T(8,128)(2,1)S(1)}, bf16[256,128]{1,0:T(8,128)(2,1)S(1)}, u32[]{:S(2)}, u32[]{:S(2)}) collective-permute-start(bf16[256,128]{1,0:T(8,128)(2,1)S(1)} %collective-permute-done.6), channel_id=1, source_target_pairs={{0,2},{2,4},{4,6},{6,8},{8,10},{10,12},{12,14},{14,16},{16,18},{18... | collective-permute-start | bytes 196616 | tf_op jit(solution)/shard_map/ppermute | solution.py:164
  81.0 7.3 %collective-permute-start.8 = (bf16[256,128]{1,0:T(8,128)(2,1)S(1)}, bf16[256,128]{1,0:T(8,128)(2,1)S(1)}, u32[]{:S(2)}, u32[]{:S(2)}) collective-permute-start(bf16[256,128]{1,0:T(8,128)(2,1)S(1)} %collective-permute-done.7), channel_id=1, source_target_pairs={{0,2},{2,4},{4,6},{6,8},{8,10},{10,12},{12,14},{14,16},{16,18},{18... | collective-permute-start | bytes 196616 | tf_op jit(solution)/shard_map/ppermute | solution.py:164
  88.3 6.7 %collective-permute-start.9 = (bf16[256,128]{1,0:T(8,128)(2,1)S(1)}, bf16[256,128]{1,0:T(8,128)(2,1)S(1)}, u32[]{:S(2)}, u32[]{:S(2)}) collective-permute-start(bf16[256,128]{1,0:T(8,128)(2,1)S(1)} %collective-permute-done.8), channel_id=1, source_target_pairs={{0,2},{2,4},{4,6},{6,8},{8,10},{10,12},{12,14},{14,16},{16,18},{18... | collective-permute-start | bytes 196616 | tf_op jit(solution)/shard_map/ppermute | solution.py:164
  95.1 6.4 %collective-permute-start.10 = (bf16[256,128]{1,0:T(8,128)(2,1)S(1)}, bf16[256,128]{1,0:T(8,128)(2,1)S(1)}, u32[]{:S(2)}, u32[]{:S(2)}) collective-permute-start(bf16[256,128]{1,0:T(8,128)(2,1)S(1)} %collective-permute-done.9), channel_id=1, source_target_pairs={{0,2},{2,4},{4,6},{6,8},{8,10},{10,12},{12,14},{14,16},{16,18},{18... | collective-permute-start | bytes 196616 | tf_op jit(solution)/shard_map/ppermute | solution.py:164
  101.5 0.6 copy-start.10
  102.1 6.4 %collective-permute-start.11 = (bf16[256,128]{1,0:T(8,128)(2,1)S(1)}, bf16[256,128]{1,0:T(8,128)(2,1)S(1)}, u32[]{:S(2)}, u32[]{:S(2)}) collective-permute-start(bf16[256,128]{1,0:T(8,128)(2,1)S(1)} %collective-permute-done.10), channel_id=1, source_target_pairs={{0,2},{2,4},{4,6},{6,8},{8,10},{10,12},{12,14},{14,16},{16,18},{18... | collective-permute-start | bytes 196616 | tf_op jit(solution)/shard_map/ppermute | solution.py:164
  108.5 6.5 %copy-start.12 = (bf16[256,128]{1,0:T(8,128)(2,1)}, bf16[256,128]{1,0:T(8,128)(2,1)S(1)}, u32[]{:S(2)}) copy-start(bf16[256,128]{1,0:T(8,128)(2,1)S(1)} %collective-permute-done.11) | copy-start | bytes 196612
  108.5 6.5 %collective-permute-start.12 = (bf16[256,128]{1,0:T(8,128)(2,1)S(1)}, bf16[256,128]{1,0:T(8,128)(2,1)}, u32[]{:S(2)}, u32[]{:S(2)}) collective-permute-start(bf16[256,128]{1,0:T(8,128)(2,1)S(1)} %collective-permute-done.11), channel_id=1, source_target_pairs={{0,2},{2,4},{4,6},{6,8},{8,10},{10,12},{12,14},{14,16},{16,18},{18... | collective-permute-start | bytes 196616 | tf_op jit(solution)/shard_map/ppermute | solution.py:164
  108.5 178.5 %all-reduce.2.cloned.1.call-start = ((), (), s32[]{:S(2)}) async-start(), calls=%async_computation.4 | async-start | bytes 1048576 | tf_op jit(solution)/shard_map/psum | solution.py:194
  115.0 6.8 %collective-permute-start.13 = (bf16[256,128]{1,0:T(8,128)(2,1)}, bf16[256,128]{1,0:T(8,128)(2,1)}, u32[]{:S(2)}, u32[]{:S(2)}) collective-permute-start(bf16[256,128]{1,0:T(8,128)(2,1)} %collective-permute-done.12), channel_id=1, source_target_pairs={{0,2},{2,4},{4,6},{6,8},{8,10},{10,12},{12,14},{14,16},{16,18},{18... | collective-permute-start | bytes 196616 | tf_op jit(solution)/shard_map/ppermute | solution.py:164
  115.7 15.4 %copy-start.13 = (bf16[256,128]{1,0:T(8,128)(2,1)S(1)}, bf16[256,128]{1,0:T(8,128)(2,1)}, u32[]{:S(2)}) copy-start(bf16[256,128]{1,0:T(8,128)(2,1)} %copy-done.12) | copy-start | bytes 196612
  115.7 15.4 %copy-start.11 = (bf16[256,128]{1,0:T(8,128)(2,1)S(1)}, bf16[256,128]{1,0:T(8,128)(2,1)}, u32[]{:S(2)}) copy-start(bf16[256,128]{1,0:T(8,128)(2,1)} %copy-done.10) | copy-start | bytes 196612
  121.8 6.7 %collective-permute-start.14 = (bf16[256,128]{1,0:T(8,128)(2,1)}, bf16[256,128]{1,0:T(8,128)(2,1)}, u32[]{:S(2)}, u32[]{:S(2)}) collective-permute-start(bf16[256,128]{1,0:T(8,128)(2,1)} %collective-permute-done.13), channel_id=1, source_target_pairs={{0,2},{2,4},{4,6},{6,8},{8,10},{10,12},{12,14},{14,16},{16,18},{18... | collective-permute-start | bytes 196616 | tf_op jit(solution)/shard_map/ppermute | solution.py:164
  135.2 4.2 %copy-start.2 = (bf16[256,128]{1,0:T(8,128)(2,1)S(1)}, bf16[256,128]{1,0:T(8,128)(2,1)}, u32[]{:S(2)}) copy-start(bf16[256,128]{1,0:T(8,128)(2,1)} %constant_dynamic-slice_fusion.6) | copy-start | bytes 196612
  212.5 19.3 %copy-start.3 = (bf16[128,2048]{1,0:T(8,128)(2,1)S(1)}, bf16[128,2048]{1,0:T(8,128)(2,1)}, u32[]{:S(2)}) copy-start(bf16[128,2048]{1,0:T(8,128)(2,1)} %param.17) | copy-start | bytes 1572868
  212.5 19.3 %copy-start.14 = (f32[2048]{0:T(1024)S(1)}, f32[2048]{0:T(1024)}, u32[]{:S(2)}) copy-start(f32[2048]{0:T(1024)} %param.19) | copy-start | bytes 24580
  214.3 103.4 %reduce-scatter.2.cloned.1.call-start = ((), (), s32[]{:S(2)}) async-start(), calls=%async_computation.6 | async-start | bytes 4456448 | tf_op jit(solution)/shard_map/reduce_scatter | solution.py:187
  235.8 1.9 copy-start.1
  245.8 1.9 copy-start.1
  256.1 1.9 copy-start.1
  266.4 1.9 copy-start.1
  275.4 9.7 %copy-start.6 = (bf16[128,2048]{1,0:T(8,128)(2,1)S(1)}, bf16[128,2048]{1,0:T(8,128)(2,1)}, u32[]{:S(2)}) copy-start(bf16[128,2048]{1,0:T(8,128)(2,1)} %param.18) | copy-start | bytes 1572868
  283.3 1.9 copy-start.7
  285.1 0.6 copy-start.22
  285.1 0.7 copy-start.20
  285.7 1.3 copy-start.4
  285.7 2.6 copy-start.18
Sparse Core Ops, SparseCore 0:
  11.3 44.9 all-gather.5
  58.4 37.4 all-gather.3
  108.6 43.0 all-gather.7
  214.4 26.1 all-reduce.1
  244.9 72.7 reduce-scatter.1
